TPU v7x, 32 devices: a whole 2x2x4 slice. The times are simulated.
32 devices in a mesh: sp: 8 (over z, y), tp: 4 (over x, core).
Axes of the slice: x: 2, y: 2, z: 4, core: 2. Of those that a mesh axis runs over, the one named last changes fastest.
Arguments:
- tokens: bfloat16 [2560, 2048], P('sp', 'tp'), may hold values from -6 to 6
- pre_gain: float32 [2, 2048], replicated, may hold values from 0.1 to 1.9
- w_value: bfloat16 [2, 2048, 2048], P(None, 'sp', 'tp'), may hold values from -0.125 to 0.125
- w_gate: bfloat16 [2, 2048, 2048], P(None, 'sp', 'tp'), may hold values from -0.125 to 0.125
- taps: float32 [2, 31, 2048], P(None, None, 'tp'), may hold values from -5 to 5
- norm_gain: float32 [2, 2048], P(None, 'tp'), may hold values from 0.1 to 1.9
- norm_shift: float32 [2, 2048], P(None, 'tp'), may hold values from -3 to 3
- w_out: bfloat16 [2, 2048, 2048], P(None, 'tp', 'sp'), may hold values from -2 to 2
- post_gain: float32 [2, 2048], P(None, 'tp'), may hold values from 0.1 to 1.9
Outputs:
- stream: bfloat16 [2560, 2048], P('sp', 'tp')
All inputs are finite; a program needn't handle non-finite values.
Results may differ from a plain program's by a relative error of at most 0.015.
Values may be sent and summed in bfloat16 or wider, within the bound.
A program may use at most 64 MiB of HBM per device.

v0:
```python
import jax
import jax.numpy as jnp
from jax import lax
from jax.sharding import PartitionSpec as P

D = 2048
CONV_WIDTH = 31
LAYERS = 2
EPSILON = 1e-06
LN_EPSILON = 1e-05


def passed_along(block, axis, distance):
    devices = range(lax.axis_size(axis))
    route = [(i - distance, i) for i in devices if i - distance in devices]
    return lax.ppermute(block, axis, route)


def local(tokens, pre_gain, w_value, w_gate, taps, norm_gain, norm_shift, w_out, post_gain):
    stream = tokens
    full_value, full_gate = (
        lax.all_gather(w_value, "sp", axis=1, tiled=True),
        lax.all_gather(w_gate, "sp", axis=1, tiled=True),
    )
    full_out = lax.all_gather(w_out, "sp", axis=2, tiled=True)
    for layer in range(LAYERS):
        whole = lax.all_gather(stream, "tp", axis=1, tiled=True)
        whole_f = whole.astype(jnp.float32)
        normed = (
            whole_f
            * lax.rsqrt(jnp.mean(whole_f * whole_f, -1, keepdims=True) + EPSILON)
            * pre_gain[layer]
        ).astype(jnp.bfloat16)
        value_mat = full_value[layer]
        gate_mat = full_gate[layer]
        out_mat = full_out[layer]
        value_proj = jnp.dot(normed, value_mat, preferred_element_type=jnp.float32)
        gate_proj = jnp.dot(normed, gate_mat, preferred_element_type=jnp.float32)
        glu_act = (value_proj * jax.nn.sigmoid(gate_proj)).astype(jnp.bfloat16)
        rows = glu_act.shape[0]
        fringe = passed_along(glu_act[rows - (CONV_WIDTH - 1) :], "sp", 1)
        padded = jnp.concatenate([fringe, glu_act], 0).astype(jnp.float32)
        conv_out = jnp.zeros(glu_act.shape, jnp.float32)
        for offset in range(CONV_WIDTH):
            conv_out = conv_out + taps[layer, offset] * padded[offset : offset + rows]
        row_sum, row_square = lax.psum(
            (jnp.sum(conv_out, -1, keepdims=True), jnp.sum(conv_out * conv_out, -1, keepdims=True)),
            "tp",
        )
        center = row_sum / D
        spread = jnp.maximum(row_square / D - center * center, 0.0)
        activated = jax.nn.silu(
            (conv_out - center) * lax.rsqrt(spread + LN_EPSILON) * norm_gain[layer]
            + norm_shift[layer]
        ).astype(jnp.bfloat16)
        terms = jnp.dot(activated, out_mat, preferred_element_type=jnp.float32)
        summed = lax.psum_scatter(terms.astype(jnp.bfloat16), "tp", scatter_dimension=1, tiled=True)
        projected = summed.astype(jnp.float32)
        out_square = lax.psum(jnp.sum(projected * projected, -1, keepdims=True), "tp")
        scale = lax.rsqrt(out_square / D + EPSILON)
        stream = (stream.astype(jnp.float32) + projected * scale * post_gain[layer]).astype(
            jnp.bfloat16
        )
    return stream


def solution(mesh):
    placed = (
        P("sp", "tp"),
        P(),
        P(None, "sp", "tp"),
        P(None, "sp", "tp"),
        P(None, None, "tp"),
        P(None, "tp"),
        P(None, "tp"),
        P(None, "tp", "sp"),
        P(None, "tp"),
    )
    return jax.shard_map(
        local, mesh=mesh, in_specs=placed, out_specs=P("sp", "tp"), check_vma=False
    )
```

profile of v0, /device:TPU:0, one launch (start us, length us, event | category | flops | bytes accessed | tf_op | source)
XLA Modules:
  0.0 377.1 jit_solution(16301794310421925368)
XLA Ops:
  6.5 0.0 all-gather.6.cloned.1.call-start
  6.5 0.7 all-gather.6.cloned.1.call-update
  7.3 0.0 all-gather.10.cloned.1.call-start
  7.3 0.7 all-gather.10.cloned.1.call-update
  8.0 0.0 all-gather.8.cloned.1.call-start
  8.1 0.7 all-gather.8.cloned.1.call-update
  8.7 0.0 all-gather.12.cloned.1.call-start
  8.8 0.5 all-gather.12.cloned.1.call-update
  9.3 0.0 reduce-scatter.3.cloned.1.call-start
  9.4 0.8 fusion.116
  10.1 0.8 fusion.113
  10.9 0.9 fusion.112
  11.8 0.9 fusion.111
  12.7 0.8 fusion.114
  13.5 16.3 %all-gather.6.cloned.1.call-done = bf16[320,2048]{1,0:T(8,128)(2,1)} async-done(((bf16[320,512]{1,0:T(8,128)(2,1)}), bf16[320,2048]{1,0:T(8,128)(2,1)}) %all-gather.6.cloned.1.call-update) | async-done | bytes 1310736 | tf_op jit(solution)/shard_map/all_gather | solution.py:27
  29.8 1.7 fusion
  31.5 73.3 %all-gather.10.cloned.1.call-done = bf16[2,2048,512]{2,1,0:T(8,128)(2,1)} async-done(((bf16[2,256,512]{2,1,0:T(8,128)(2,1)}), bf16[2,2048,512]{2,1,0:T(8,128)(2,1)}) %all-gather.10.cloned.1.call-update) | async-done | bytes 4194320 | tf_op jit(solution)/shard_map/all_gather | solution.py:23
  104.8 0.0 copy-start.1
  104.8 3.1 fusion.20
  107.9 0.0 copy-start.4
  107.9 70.4 %all-gather.8.cloned.1.call-done = bf16[2,2048,512]{2,1,0:T(8,128)(2,1)} async-done(((bf16[2,256,512]{2,1,0:T(8,128)(2,1)}), bf16[2,2048,512]{2,1,0:T(8,128)(2,1)}) %all-gather.8.cloned.1.call-update) | async-done | bytes 4194320 | tf_op jit(solution)/shard_map/all_gather | solution.py:22
  178.3 0.0 copy-done.1
  178.3 2.5 fusion.19
  180.8 2.5 collective-permute-start
  183.3 0.0 copy-done.4
  183.3 1.6 collective-permute-done
  184.9 0.1 maximum_convert_fusion
  185.0 3.2 fusion.107
  188.2 6.1 %all-reduce.1 = (f32[320,1]{0,1:T(1,128)S(1)}, f32[320,1]{0,1:T(1,128)S(1)}) all-reduce(f32[320,1]{0,1:T(1,128)S(1)} %broadcast_in_dim.20, f32[320,1]{0,1:T(1,128)S(1)} %broadcast_in_dim.21), channel_id=1, replica_groups=mesh['sp'=8,'tp'=4] {'tp'}, use_global_device_ids=true, to_apply=%region_2.0 | all-reduce | flops 640 | bytes 5120 | tf_op jit(solution)/shard_map/psum | solution.py:46
  194.3 59.2 %all-gather.12.cloned.1.call-done = bf16[2,512,2048]{2,1,0:T(8,128)(2,1)} async-done(((bf16[2,512,256]{2,1,0:T(8,128)(2,1)}), bf16[2,512,2048]{2,1,0:T(8,128)(2,1)}) %all-gather.12.cloned.1.call-update) | async-done | bytes 4194320 | tf_op jit(solution)/shard_map/all_gather | solution.py:25
  253.4 0.0 copy-start.5
  253.5 3.8 %convolution_convert_fusion.1 = bf16[320,2048]{1,0:T(8,128)(2,1)} fusion(bf16[2,512,2048]{2,1,0:T(8,128)(2,1)} %all-gather.12.cloned.1.call-done, f32[320,512]{1,0:T(8,128)S(1)} %get-tuple-element.18, f32[512]{0:T(512)S(1)} %bitcast.183, f32[512]{0:T(512)S(1)} %bitcast.182, f32[320]{0:T(512)S(1)} %get-tuple-element.12, f32[320]{0:T(512)S(1)} %get-tuple-element.11), kind=kOutput, calls=%fused_computation.5 | convolution fusion | flops 673218560 | bytes 4069888 | tf_op jit(solution)/shard_map/dot_general | solution.py:56
  257.2 0.0 reduce-scatter.3.cloned.1.call-update
  257.3 0.0 all-gather.14.cloned.1.call-start
  257.3 0.0 copy-done.5
  257.3 24.7 %reduce-scatter.3.cloned.1.call-done = bf16[320,512]{1,0:T(8,128)(2,1)} async-done(((bf16[320,2048]{1,0:T(8,128)(2,1)}), bf16[320,512]{1,0:T(8,128)(2,1)}) %reduce-scatter.3.cloned.1.call-update) | async-done | bytes 327696 | tf_op jit(solution)/shard_map/reduce_scatter | solution.py:57
  282.0 1.1 fusion.22
  283.2 5.8 %psum.44 = f32[320,1]{0,1:T(1,128)S(1)} all-reduce(f32[320,1]{0,1:T(1,128)S(1)} %broadcast_in_dim.22), channel_id=1, replica_groups=mesh['sp'=8,'tp'=4] {'tp'}, use_global_device_ids=true, to_apply=%region_7.8 | all-reduce | flops 320 | bytes 2560 | tf_op jit(solution)/shard_map/psum | solution.py:59
  288.9 0.0 copy-done.3
  289.0 1.9 fusion.25
  290.8 0.0 all-gather.14.cloned.1.call-update
  290.9 0.0 reduce-scatter.5.cloned.1.call-start
  290.9 18.9 %all-gather.14.cloned.1.call-done = bf16[320,2048]{1,0:T(8,128)(2,1)} async-done(((bf16[320,512]{1,0:T(8,128)(2,1)}), bf16[320,2048]{1,0:T(8,128)(2,1)}) %all-gather.14.cloned.1.call-update) | async-done | bytes 1310736 | tf_op jit(solution)/shard_map/all_gather | solution.py:27
  309.8 1.7 fusion.3
  311.5 0.0 copy-start.2
  311.5 0.0 copy-start.6
  311.5 3.1 fusion.21
  314.6 0.0 copy-done.2
  314.6 0.5 copy-done.6
  315.1 0.9 fusion.18
  316.0 3.4 collective-permute-start.1
  319.4 0.9 fusion.110
  320.3 0.7 collective-permute-done.1
  321.0 0.1 maximum_convert_fusion.1
  321.1 3.2 fusion.106
  324.3 6.0 %all-reduce = (f32[320,1]{0,1:T(1,128)S(1)}, f32[320,1]{0,1:T(1,128)S(1)}) all-reduce(f32[320,1]{0,1:T(1,128)S(1)} %broadcast_in_dim.23, f32[320,1]{0,1:T(1,128)S(1)} %broadcast_in_dim.24), channel_id=1, replica_groups=mesh['sp'=8,'tp'=4] {'tp'}, use_global_device_ids=true, to_apply=%region_10.11 | all-reduce | flops 640 | bytes 5120 | tf_op jit(solution)/shard_map/psum | solution.py:46
  330.3 0.0 copy-start
  330.3 3.7 convolution_convert_fusion
  334.0 0.0 reduce-scatter.5.cloned.1.call-update
  334.0 27.4 %reduce-scatter.5.cloned.1.call-done = bf16[320,512]{1,0:T(8,128)(2,1)} async-done(((bf16[320,2048]{1,0:T(8,128)(2,1)}), bf16[320,512]{1,0:T(8,128)(2,1)}) %reduce-scatter.5.cloned.1.call-update) | async-done | bytes 327696 | tf_op jit(solution)/shard_map/reduce_scatter | solution.py:57
  361.4 1.1 fusion.26
  362.5 5.8 %psum.47 = f32[320,1]{0,1:T(1,128)S(1)} all-reduce(f32[320,1]{0,1:T(1,128)S(1)} %broadcast_in_dim.25), channel_id=1, replica_groups=mesh['sp'=8,'tp'=4] {'tp'}, use_global_device_ids=true, to_apply=%region_15.16 | all-reduce | flops 320 | bytes 2560 | tf_op jit(solution)/shard_map/psum | solution.py:59
  368.3 0.0 copy-done
  368.3 1.9 fusion.29
  (17 shorter events, 0.2 us)
Async XLA Ops:
  6.5 23.3 %all-gather.6.cloned.1.call-start = ((), (), s32[]{:S(2)}) async-start(), calls=%async_computation.2 | async-start | bytes 1638400 | tf_op jit(solution)/shard_map/all_gather | solution.py:27
  7.3 97.5 %all-gather.10.cloned.1.call-start = ((), (), s32[]{:S(2)}) async-start(), calls=%async_computation.4 | async-start | bytes 4718592 | tf_op jit(solution)/shard_map/all_gather | solution.py:23
  8.0 170.3 %all-gather.8.cloned.1.call-start = ((), (), s32[]{:S(2)}) async-start(), calls=%async_computation.3 | async-start | bytes 4718592 | tf_op jit(solution)/shard_map/all_gather | solution.py:22
  8.7 244.7 %all-gather.12.cloned.1.call-start = ((), (), s32[]{:S(2)}) async-start(), calls=%async_computation.5 | async-start | bytes 4718592 | tf_op jit(solution)/shard_map/all_gather | solution.py:25
  9.3 272.7 %reduce-scatter.3.cloned.1.call-start = ((), (), s32[]{:S(2)}) async-start(), calls=%async_computation.6 | async-start | bytes 1638400 | tf_op jit(solution)/shard_map/reduce_scatter | solution.py:57
  104.8 73.5 %copy-start.1 = (bf16[320,2048]{1,0:T(8,128)(2,1)S(1)}, bf16[320,2048]{1,0:T(8,128)(2,1)}, u32[]{:S(2)}) copy-start(bf16[320,2048]{1,0:T(8,128)(2,1)} %all-gather.6.cloned.1.call-done) | copy-start | bytes 3932164
  107.9 75.4 %copy-start.4 = (f32[2,512]{1,0:T(2,128)S(1)}, f32[2,512]{1,0:T(2,128)}, u32[]{:S(2)}) copy-start(f32[2,512]{1,0:T(2,128)} %param.15) | copy-start | bytes 12292
  180.8 4.0 %collective-permute-start = (bf16[30,512]{1,0:T(8,128)(2,1)S(1)}, bf16[30,512]{1,0:T(8,128)(2,1)S(1)}, u32[]{:S(2)}, u32[]{:S(2)}) collective-permute-start(bf16[30,512]{1,0:T(8,128)(2,1)S(1)} %slice.562), channel_id=1, source_target_pairs={{0,4},{4,8},{8,12},{12,16},{16,20},{20,24},{24,28},{1,5},{5,9},{9,... | collective-permute-start | bytes 92168 | tf_op jit(solution)/shard_map/ppermute | solution.py:16
  253.4 3.9 %copy-start.5 = (f32[2,512]{1,0:T(2,128)S(1)}, f32[2,512]{1,0:T(2,128)}, u32[]{:S(2)}) copy-start(f32[2,512]{1,0:T(2,128)} %param.17) | copy-start | bytes 12292
  253.4 35.5 %copy-start.3 = (bf16[320,512]{1,0:T(8,128)(2,1)S(1)}, bf16[320,512]{1,0:T(8,128)(2,1)}, u32[]{:S(2)}) copy-start(bf16[320,512]{1,0:T(8,128)(2,1)} %param.9) | copy-start | bytes 983044
  257.3 52.5 %all-gather.14.cloned.1.call-start = ((), (), s32[]{:S(2)}) async-start(), calls=%async_computation.7 | async-start | bytes 1638400 | tf_op jit(solution)/shard_map/all_gather | solution.py:27
  290.9 70.5 %reduce-scatter.5.cloned.1.call-start = ((), (), s32[]{:S(2)}) async-start(), calls=%async_computation.8 | async-start | bytes 1638400 | tf_op jit(solution)/shard_map/reduce_scatter | solution.py:57
  311.5 3.1 copy-start.2
  311.5 3.6 copy-start.6
  316.0 5.0 %collective-permute-start.1 = (bf16[30,512]{1,0:T(8,128)(2,1)S(1)}, bf16[30,512]{1,0:T(8,128)(2,1)S(1)}, u32[]{:S(2)}, u32[]{:S(2)}) collective-permute-start(bf16[30,512]{1,0:T(8,128)(2,1)S(1)} %slice.597), channel_id=1, source_target_pairs={{0,4},{4,8},{8,12},{12,16},{16,20},{20,24},{24,28},{1,5},{5,9},{9,... | collective-permute-start | bytes 92168 | tf_op jit(solution)/shard_map/ppermute | solution.py:16
  330.3 38.1 %copy-start = (bf16[320,512]{1,0:T(8,128)(2,1)S(1)}, bf16[320,512]{1,0:T(8,128)(2,1)}, u32[]{:S(2)}) copy-start(bf16[320,512]{1,0:T(8,128)(2,1)} %fusion.25) | copy-start | bytes 983044
Sparse Core Ops, SparseCore 0:
  8.9 20.8 all-gather.5
  32.0 72.7 all-gather.9
  107.0 71.2 all-gather.7
  180.2 73.1 all-gather.11
  257.4 24.5 reduce-scatter.2
  291.0 18.7 all-gather.13
  334.1 27.2 reduce-scatter.4
where the time goes:
time: 378 us; the launch traced here: 377 us
  waiting for transfers between devices  295 us (78%)
  blocking collectives  23.5 us (6%)
  matrix products  17 us (4%)
  other arithmetic  16 us (4%)
  between operations  13.7 us (4%)
  starting transfers between devices  6.07 us (2%)
  local copies, waits for them, and re-layouts  5.61 us (1%)
    all_gather x1, waiting for transfers between devices, local(): lax.all_gather(w_gate, 'sp', axis=1, tiled=True)  73.3 us
    all_gather x1, waiting for transfers between devices, local(): lax.all_gather(w_value, 'sp', axis=1, tiled=True)  70.4 us
    all_gather x1, waiting for transfers between devices, local(): full_out = lax.all_gather(w_out, 'sp', axis=2, tiled=True)  59.2 us
    reduce_scatter x2, waiting for transfers between devices, local(): lax.psum_scatter(terms.astype(jnp.bfloat16), 'tp', scatter_dimension=1, t...  52.1 us
    all_gather x2, waiting for transfers between devices, local(): whole = lax.all_gather(stream, 'tp', axis=1, tiled=True)  35.2 us
    psum x2, blocking collectives, local(): lax.psum((jnp.sum(conv_out, -1, keepdims=True), jnp.sum(conv_out * conv_o...  12 us
    psum x2, blocking collectives, local(): lax.psum(jnp.sum(projected * projected, -1, keepdims=True), 'tp')  11.5 us
  transfers between devices with their start and end apart: 9, of which 9 were waited for; matrix products, arithmetic and copies ran while one was open for 4% of the time, Pallas kernels for 0%

commit v1 on v0

--- a/solution.py
+++ b/solution.py
@@ -24,7 +24,14 @@
     )
     full_out = lax.all_gather(w_out, "sp", axis=2, tiled=True)
     for layer in range(LAYERS):
-        whole = lax.all_gather(stream, "tp", axis=1, tiled=True)
+        ring = [stream]
+        for hop in range(3):
+            ring.append(lax.ppermute(ring[-1], "tp", [(dev, (dev + 1) % 4) for dev in range(4)]))
+        whole = jnp.roll(
+            jnp.concatenate(ring[::-1], axis=1),
+            (lax.axis_index("tp") + 1) * ring[0].shape[1],
+            axis=1,
+        )
         whole_f = whole.astype(jnp.float32)
         normed = (
             whole_f

time: 378 us -> 359 us (0.950)
  waiting for transfers between devices: 295 us -> 274 us
  other arithmetic: 16 us -> 19.9 us
    all_gather x2 -> x0, waiting for transfers between devices: 35.2 us -> none  [local(): whole = lax.all_gather(stream, 'tp', axis=1, tiled=True)]
    ppermute x0 -> x6, waiting for transfers between devices: none -> 35.2 us  [local(): lax.ppermute(ring[-1], 'tp', [(dev, (dev + 1) % 4) for dev in range(4)])]
    all_gather x1, waiting for transfers between devices: 73.3 us -> 51.6 us  [local(): lax.all_gather(w_gate, 'sp', axis=1, tiled=True)]
    reduce_sum x2, other arithmetic: 3.33 us -> 7.93 us  [local(): jnp.mean(whole_f * whole_f, -1, keepdims=True) + EPSILON]
  transfers between devices with their start and end apart: 9 -> 13, of which waited for: 9 -> 13; matrix products, arithmetic and copies ran while one was open for 4% -> 5% of each run, Pallas kernels for 0% -> 0%
where the time goes in v1:
time: 359 us
  waiting for transfers between devices  274 us (76%)
  blocking collectives  23.3 us (6%)
  other arithmetic  19.9 us (6%)
  matrix products  16.2 us (5%)
  between operations  13.4 us (4%)
  starting transfers between devices  7.02 us (2%)
  local copies, waits for them, and re-layouts  5.19 us (1%)
    all_gather x1, waiting for transfers between devices, local(): lax.all_gather(w_value, 'sp', axis=1, tiled=True)  70.9 us
    all_gather x1, waiting for transfers between devices, local(): full_out = lax.all_gather(w_out, 'sp', axis=2, tiled=True)  59.3 us
    reduce_scatter x2, waiting for transfers between devices, local(): lax.psum_scatter(terms.astype(jnp.bfloat16), 'tp', scatter_dimension=1, t...  52.5 us
    all_gather x1, waiting for transfers between devices, local(): lax.all_gather(w_gate, 'sp', axis=1, tiled=True)  51.6 us
    ppermute x6, waiting for transfers between devices, local(): lax.ppermute(ring[-1], 'tp', [(dev, (dev + 1) % 4) for dev in range(4)])  35.2 us
    psum x2, blocking collectives, local(): lax.psum((jnp.sum(conv_out, -1, keepdims=True), jnp.sum(conv_out * conv_o...  11.7 us
    psum x2, blocking collectives, local(): lax.psum(jnp.sum(projected * projected, -1, keepdims=True), 'tp')  11.5 us
    reduce_sum x2, other arithmetic, local(): jnp.mean(whole_f * whole_f, -1, keepdims=True) + EPSILON  7.93 us
  transfers between devices with their start and end apart: 13, of which 13 were waited for; matrix products, arithmetic and copies ran while one was open for 5% of the time, Pallas kernels for 0%

profile of v1, /device:TPU:0, one launch (start us, length us, event | category | flops | bytes accessed | tf_op | source)
XLA Modules:
  0.0 358.5 jit_solution(8951229100149773190)
XLA Ops:
  6.5 0.0 all-gather.6.cloned.1.call-start
  6.5 0.7 all-gather.6.cloned.1.call-update
  7.3 0.0 all-gather.4.cloned.1.call-start
  7.3 0.7 all-gather.4.cloned.1.call-update
  8.0 0.0 all-gather.8.cloned.1.call-start
  8.1 0.7 all-gather.8.cloned.1.call-update
  8.7 0.0 reduce-scatter.3.cloned.1.call-start
  8.8 0.5 collective-permute-start
  9.3 0.8 fusion.130
  10.1 6.1 %collective-permute-done = bf16[320,512]{1,0:T(8,128)(2,1)S(1)} collective-permute-done((bf16[320,512]{1,0:T(8,128)(2,1)}, bf16[320,512]{1,0:T(8,128)(2,1)S(1)}, u32[]{:S(2)}, u32[]{:S(2)}) %collective-permute-start) | collective-permute-done | bytes 327712 | tf_op jit(solution)/shard_map/ppermute | solution.py:29
  16.2 0.0 collective-permute-start.1
  16.3 0.8 fusion.129
  17.0 0.9 fusion.128
  17.9 4.8 %collective-permute-done.1 = bf16[320,512]{1,0:T(8,128)(2,1)S(1)} collective-permute-done((bf16[320,512]{1,0:T(8,128)(2,1)S(1)}, bf16[320,512]{1,0:T(8,128)(2,1)S(1)}, u32[]{:S(2)}, u32[]{:S(2)}) %collective-permute-start.1) | collective-permute-done | bytes 327712 | tf_op jit(solution)/shard_map/ppermute | solution.py:29
  22.7 0.0 collective-permute-start.2
  22.7 0.8 fusion.132
  23.5 0.9 fusion.127
  24.4 4.8 %collective-permute-done.2 = bf16[320,512]{1,0:T(8,128)(2,1)S(1)} collective-permute-done((bf16[320,512]{1,0:T(8,128)(2,1)S(1)}, bf16[320,512]{1,0:T(8,128)(2,1)S(1)}, u32[]{:S(2)}, u32[]{:S(2)}) %collective-permute-start.2) | collective-permute-done | bytes 327712 | tf_op jit(solution)/shard_map/ppermute | solution.py:29
  29.2 4.2 %fusion = (f32[320]{0:T(512)S(1)}, bf16[320,2048]{1,0:T(8,128)(2,1)S(1)}) fusion(s32[]{:T(128)S(6)} %select_n.13, bf16[320,512]{1,0:T(8,128)(2,1)} %param.11, bf16[320,512]{1,0:T(8,128)(2,1)S(1)} %collective-permute-done, bf16[320,512]{1,0:T(8,128)(2,1)S(1)} %collective-permute-done.1, bf16[320,512]{1,0:T(8,128)(2,1)S(1)} %collective-permute-done.2), kind=kLoop, calls=%fused_computation.6 | loop fusion | flops 12451520 | bytes 2622724 | tf_op jit(solution)/shard_map/reduce_sum | solution.py:38
  33.5 51.6 %all-gather.6.cloned.1.call-done = bf16[2,2048,512]{2,1,0:T(8,128)(2,1)} async-done(((bf16[2,256,512]{2,1,0:T(8,128)(2,1)}), bf16[2,2048,512]{2,1,0:T(8,128)(2,1)}) %all-gather.6.cloned.1.call-update) | async-done | bytes 4194320 | tf_op jit(solution)/shard_map/all_gather | solution.py:23
  85.0 2.6 fusion.34
  87.6 0.0 copy-start.1
  87.7 70.9 %all-gather.4.cloned.1.call-done = bf16[2,2048,512]{2,1,0:T(8,128)(2,1)} async-done(((bf16[2,256,512]{2,1,0:T(8,128)(2,1)}), bf16[2,2048,512]{2,1,0:T(8,128)(2,1)}) %all-gather.4.cloned.1.call-update) | async-done | bytes 4194320 | tf_op jit(solution)/shard_map/all_gather | solution.py:22
  158.6 2.5 fusion.33
  161.1 2.4 collective-permute-start.3
  163.6 0.0 copy-done.1
  163.6 1.6 collective-permute-done.3
  165.1 0.1 maximum_convert_fusion
  165.2 3.2 fusion.121
  168.5 6.1 %all-reduce.1 = (f32[320,1]{0,1:T(1,128)S(1)}, f32[320,1]{0,1:T(1,128)S(1)}) all-reduce(f32[320,1]{0,1:T(1,128)S(1)} %broadcast_in_dim.20, f32[320,1]{0,1:T(1,128)S(1)} %broadcast_in_dim.21), channel_id=1, replica_groups=mesh['sp'=8,'tp'=4] {'tp'}, use_global_device_ids=true, to_apply=%region_2.4 | all-reduce | flops 640 | bytes 5120 | tf_op jit(solution)/shard_map/psum | solution.py:53
  174.6 59.3 %all-gather.8.cloned.1.call-done = bf16[2,512,2048]{2,1,0:T(8,128)(2,1)} async-done(((bf16[2,512,256]{2,1,0:T(8,128)(2,1)}), bf16[2,512,2048]{2,1,0:T(8,128)(2,1)}) %all-gather.8.cloned.1.call-update) | async-done | bytes 4194320 | tf_op jit(solution)/shard_map/all_gather | solution.py:25
  233.8 0.0 copy-start.2
  233.8 3.8 %convolution_convert_fusion.1 = bf16[320,2048]{1,0:T(8,128)(2,1)} fusion(bf16[2,512,2048]{2,1,0:T(8,128)(2,1)} %all-gather.8.cloned.1.call-done, f32[320,512]{1,0:T(8,128)S(1)} %get-tuple-element.21, f32[512]{0:T(512)S(1)} %bitcast.183, f32[512]{0:T(512)S(1)} %bitcast.182, f32[320]{0:T(512)S(1)} %get-tuple-element.13, f32[320]{0:T(512)S(1)} %get-tuple-element.12), kind=kOutput, calls=%fused_computation.5 | convolution fusion | flops 673218560 | bytes 4069888 | tf_op jit(solution)/shard_map/dot_general | solution.py:63
  237.6 0.0 reduce-scatter.3.cloned.1.call-update
  237.7 0.0 reduce-scatter.5.cloned.1.call-start
  237.7 0.0 copy-done.2
  237.7 24.7 %reduce-scatter.3.cloned.1.call-done = bf16[320,512]{1,0:T(8,128)(2,1)} async-done(((bf16[320,2048]{1,0:T(8,128)(2,1)}), bf16[320,512]{1,0:T(8,128)(2,1)}) %reduce-scatter.3.cloned.1.call-update) | async-done | bytes 327696 | tf_op jit(solution)/shard_map/reduce_scatter | solution.py:64
  262.4 1.1 fusion.36
  263.5 5.8 %psum.44 = f32[320,1]{0,1:T(1,128)S(1)} all-reduce(f32[320,1]{0,1:T(1,128)S(1)} %broadcast_in_dim.22), channel_id=1, replica_groups=mesh['sp'=8,'tp'=4] {'tp'}, use_global_device_ids=true, to_apply=%region_7.9 | all-reduce | flops 320 | bytes 2560 | tf_op jit(solution)/shard_map/psum | solution.py:66
  269.3 0.0 copy-done
  269.3 1.2 fusion.39
  270.5 0.1 collective-permute-start.4
  270.6 6.5 %collective-permute-done.4 = bf16[320,512]{1,0:T(8,128)(2,1)S(1)} collective-permute-done((bf16[320,512]{1,0:T(8,128)(2,1)S(1)}, bf16[320,512]{1,0:T(8,128)(2,1)S(1)}, u32[]{:S(2)}, u32[]{:S(2)}) %collective-permute-start.4) | collective-permute-done | bytes 327712 | tf_op jit(solution)/shard_map/ppermute | solution.py:29
  277.1 0.0 collective-permute-start.5
  277.1 6.5 %collective-permute-done.5 = bf16[320,512]{1,0:T(8,128)(2,1)S(1)} collective-permute-done((bf16[320,512]{1,0:T(8,128)(2,1)S(1)}, bf16[320,512]{1,0:T(8,128)(2,1)S(1)}, u32[]{:S(2)}, u32[]{:S(2)}) %collective-permute-start.5) | collective-permute-done | bytes 327712 | tf_op jit(solution)/shard_map/ppermute | solution.py:29
  283.6 0.0 collective-permute-start.6
  283.6 6.5 %collective-permute-done.6 = bf16[320,512]{1,0:T(8,128)(2,1)S(1)} collective-permute-done((bf16[320,512]{1,0:T(8,128)(2,1)S(1)}, bf16[320,512]{1,0:T(8,128)(2,1)S(1)}, u32[]{:S(2)}, u32[]{:S(2)}) %collective-permute-start.6) | collective-permute-done | bytes 327712 | tf_op jit(solution)/shard_map/ppermute | solution.py:29
  290.1 3.7 %fusion.3 = (f32[320]{0:T(512)S(1)}, bf16[320,2048]{1,0:T(8,128)(2,1)S(1)}) fusion(s32[]{:T(128)S(6)} %select_n.13, bf16[320,512]{1,0:T(8,128)(2,1)S(1)} %fusion.39, bf16[320,512]{1,0:T(8,128)(2,1)S(1)} %collective-permute-done.4, bf16[320,512]{1,0:T(8,128)(2,1)S(1)} %collective-permute-done.5, bf16[320,512]{1,0:T(8,128)(2,1)S(1)} %collective-permute-done.6), kind=kLoop, calls=%fused_computation.9 | loop fusion | flops 12451520 | bytes 2622724 | tf_op jit(solution)/shard_map/reduce_sum | solution.py:38
  293.8 0.0 copy-start.3
  293.8 2.7 fusion.35
  296.5 0.1 copy-done.3
  296.6 0.9 fusion.32
  297.5 3.8 %collective-permute-start.7 = (bf16[30,512]{1,0:T(8,128)(2,1)S(1)}, bf16[30,512]{1,0:T(8,128)(2,1)S(1)}, u32[]{:S(2)}, u32[]{:S(2)}) collective-permute-start(bf16[30,512]{1,0:T(8,128)(2,1)S(1)} %slice.597), channel_id=1, source_target_pairs={{0,4},{4,8},{8,12},{12,16},{16,20},{20,24},{24,28},{1,5},{5,9},{9,... | collective-permute-start | bytes 92168 | tf_op jit(solution)/shard_map/ppermute | solution.py:16
  301.3 0.9 fusion.126
  302.2 0.5 collective-permute-done.7
  302.7 0.1 maximum_convert_fusion.1
  302.8 3.2 fusion.120
  306.0 5.7 %all-reduce = (f32[320,1]{0,1:T(1,128)S(1)}, f32[320,1]{0,1:T(1,128)S(1)}) all-reduce(f32[320,1]{0,1:T(1,128)S(1)} %broadcast_in_dim.23, f32[320,1]{0,1:T(1,128)S(1)} %broadcast_in_dim.24), channel_id=1, replica_groups=mesh['sp'=8,'tp'=4] {'tp'}, use_global_device_ids=true, to_apply=%region_10.12 | all-reduce | flops 640 | bytes 5120 | tf_op jit(solution)/shard_map/psum | solution.py:53
  311.7 3.7 %convolution_convert_fusion = bf16[320,2048]{1,0:T(8,128)(2,1)} fusion(bf16[2,512,2048]{2,1,0:T(8,128)(2,1)} %all-gather.8.cloned.1.call-done, f32[320,512]{1,0:T(8,128)S(1)} %get-tuple-element.18, f32[512]{0:T(512)S(1)} %bitcast.181, f32[512]{0:T(512)S(1)} %bitcast.180, f32[320]{0:T(512)S(1)} %get-tuple-element.11, f32[320]{0:T(512)S(1)} %get-tuple-element.10), kind=kOutput, calls=%fused_computation.4 | convolution fusion | flops 673218560 | bytes 4069888 | tf_op jit(solution)/shard_map/dot_general | solution.py:63
  315.3 0.0 reduce-scatter.5.cloned.1.call-update
  315.4 27.8 %reduce-scatter.5.cloned.1.call-done = bf16[320,512]{1,0:T(8,128)(2,1)} async-done(((bf16[320,2048]{1,0:T(8,128)(2,1)}), bf16[320,512]{1,0:T(8,128)(2,1)}) %reduce-scatter.5.cloned.1.call-update) | async-done | bytes 327696 | tf_op jit(solution)/shard_map/reduce_scatter | solution.py:64
  343.2 1.1 fusion.40
  344.3 5.8 %psum.47 = f32[320,1]{0,1:T(1,128)S(1)} all-reduce(f32[320,1]{0,1:T(1,128)S(1)} %broadcast_in_dim.25), channel_id=1, replica_groups=mesh['sp'=8,'tp'=4] {'tp'}, use_global_device_ids=true, to_apply=%region_15.17 | all-reduce | flops 320 | bytes 2560 | tf_op jit(solution)/shard_map/psum | solution.py:66
  350.1 1.9 fusion.43
  (17 shorter events, 0.2 us)
Async XLA Ops:
  6.5 78.5 %all-gather.6.cloned.1.call-start = ((), (), s32[]{:S(2)}) async-start(), calls=%async_computation.3 | async-start | bytes 4718592 | tf_op jit(solution)/shard_map/all_gather | solution.py:23
  7.3 151.3 %all-gather.4.cloned.1.call-start = ((), (), s32[]{:S(2)}) async-start(), calls=%async_computation.2 | async-start | bytes 4718592 | tf_op jit(solution)/shard_map/all_gather | solution.py:22
  8.0 225.8 %all-gather.8.cloned.1.call-start = ((), (), s32[]{:S(2)}) async-start(), calls=%async_computation.4 | async-start | bytes 4718592 | tf_op jit(solution)/shard_map/all_gather | solution.py:25
  8.7 253.7 %reduce-scatter.3.cloned.1.call-start = ((), (), s32[]{:S(2)}) async-start(), calls=%async_computation.5 | async-start | bytes 1638400 | tf_op jit(solution)/shard_map/reduce_scatter | solution.py:64
  8.8 7.4 %collective-permute-start = (bf16[320,512]{1,0:T(8,128)(2,1)}, bf16[320,512]{1,0:T(8,128)(2,1)S(1)}, u32[]{:S(2)}, u32[]{:S(2)}) collective-permute-start(bf16[320,512]{1,0:T(8,128)(2,1)} %param.11), channel_id=1, source_target_pairs={{0,1},{1,2},{2,3},{3,0},{4,5},{5,6},{6,7},{7,4},{8,9},{9,10},{10,1... | collective-permute-start | bytes 983048 | tf_op jit(solution)/shard_map/ppermute | solution.py:29
  16.2 6.5 %collective-permute-start.1 = (bf16[320,512]{1,0:T(8,128)(2,1)S(1)}, bf16[320,512]{1,0:T(8,128)(2,1)S(1)}, u32[]{:S(2)}, u32[]{:S(2)}) collective-permute-start(bf16[320,512]{1,0:T(8,128)(2,1)S(1)} %collective-permute-done), channel_id=1, source_target_pairs={{0,1},{1,2},{2,3},{3,0},{4,5},{5,6},{6,7},{7,4},{8,9},{9,10},{10,1... | collective-permute-start | bytes 983048 | tf_op jit(solution)/shard_map/ppermute | solution.py:29
  22.7 6.5 %collective-permute-start.2 = (bf16[320,512]{1,0:T(8,128)(2,1)S(1)}, bf16[320,512]{1,0:T(8,128)(2,1)S(1)}, u32[]{:S(2)}, u32[]{:S(2)}) collective-permute-start(bf16[320,512]{1,0:T(8,128)(2,1)S(1)} %collective-permute-done.1), channel_id=1, source_target_pairs={{0,1},{1,2},{2,3},{3,0},{4,5},{5,6},{6,7},{7,4},{8,9},{9,10},{10,1... | collective-permute-start | bytes 983048 | tf_op jit(solution)/shard_map/ppermute | solution.py:29
  87.6 75.9 %copy-start.1 = (f32[2,512]{1,0:T(2,128)S(1)}, f32[2,512]{1,0:T(2,128)}, u32[]{:S(2)}) copy-start(f32[2,512]{1,0:T(2,128)} %param.17) | copy-start | bytes 12292
  161.1 4.0 %collective-permute-start.3 = (bf16[30,512]{1,0:T(8,128)(2,1)S(1)}, bf16[30,512]{1,0:T(8,128)(2,1)S(1)}, u32[]{:S(2)}, u32[]{:S(2)}) collective-permute-start(bf16[30,512]{1,0:T(8,128)(2,1)S(1)} %slice.562), channel_id=1, source_target_pairs={{0,4},{4,8},{8,12},{12,16},{16,20},{20,24},{24,28},{1,5},{5,9},{9,... | collective-permute-start | bytes 92168 | tf_op jit(solution)/shard_map/ppermute | solution.py:16
  233.8 3.9 %copy-start.2 = (f32[2,512]{1,0:T(2,128)S(1)}, f32[2,512]{1,0:T(2,128)}, u32[]{:S(2)}) copy-start(f32[2,512]{1,0:T(2,128)} %param.19) | copy-start | bytes 12292
  233.8 35.5 %copy-start = (bf16[320,512]{1,0:T(8,128)(2,1)S(1)}, bf16[320,512]{1,0:T(8,128)(2,1)}, u32[]{:S(2)}) copy-start(bf16[320,512]{1,0:T(8,128)(2,1)} %param.11) | copy-start | bytes 983044
  237.7 105.5 %reduce-scatter.5.cloned.1.call-start = ((), (), s32[]{:S(2)}) async-start(), calls=%async_computation.6 | async-start | bytes 1638400 | tf_op jit(solution)/shard_map/reduce_scatter | solution.py:64
  270.5 6.6 %collective-permute-start.4 = (bf16[320,512]{1,0:T(8,128)(2,1)S(1)}, bf16[320,512]{1,0:T(8,128)(2,1)S(1)}, u32[]{:S(2)}, u32[]{:S(2)}) collective-permute-start(bf16[320,512]{1,0:T(8,128)(2,1)S(1)} %fusion.39), channel_id=1, source_target_pairs={{0,1},{1,2},{2,3},{3,0},{4,5},{5,6},{6,7},{7,4},{8,9},{9,10},{10,1... | collective-permute-start | bytes 983048 | tf_op jit(solution)/shard_map/ppermute | solution.py:29
  277.1 6.5 %collective-permute-start.5 = (bf16[320,512]{1,0:T(8,128)(2,1)S(1)}, bf16[320,512]{1,0:T(8,128)(2,1)S(1)}, u32[]{:S(2)}, u32[]{:S(2)}) collective-permute-start(bf16[320,512]{1,0:T(8,128)(2,1)S(1)} %collective-permute-done.4), channel_id=1, source_target_pairs={{0,1},{1,2},{2,3},{3,0},{4,5},{5,6},{6,7},{7,4},{8,9},{9,10},{10,1... | collective-permute-start | bytes 983048 | tf_op jit(solution)/shard_map/ppermute | solution.py:29
  283.6 6.5 %collective-permute-start.6 = (bf16[320,512]{1,0:T(8,128)(2,1)S(1)}, bf16[320,512]{1,0:T(8,128)(2,1)S(1)}, u32[]{:S(2)}, u32[]{:S(2)}) collective-permute-start(bf16[320,512]{1,0:T(8,128)(2,1)S(1)} %collective-permute-done.5), channel_id=1, source_target_pairs={{0,1},{1,2},{2,3},{3,0},{4,5},{5,6},{6,7},{7,4},{8,9},{9,10},{10,1... | collective-permute-start | bytes 983048 | tf_op jit(solution)/shard_map/ppermute | solution.py:29
  293.8 2.8 copy-start.3
  297.5 5.2 %collective-permute-start.7 = (bf16[30,512]{1,0:T(8,128)(2,1)S(1)}, bf16[30,512]{1,0:T(8,128)(2,1)S(1)}, u32[]{:S(2)}, u32[]{:S(2)}) collective-permute-start(bf16[30,512]{1,0:T(8,128)(2,1)S(1)} %slice.597), channel_id=1, source_target_pairs={{0,4},{4,8},{8,12},{12,16},{16,20},{20,24},{24,28},{1,5},{5,9},{9,... | collective-permute-start | bytes 92168 | tf_op jit(solution)/shard_map/ppermute | solution.py:16
Sparse Core Ops, SparseCore 0:
  9.5 75.4 all-gather.5
  87.2 71.2 all-gather.3
  160.6 73.1 all-gather.7
  237.8 24.5 reduce-scatter.2
  315.5 27.6 reduce-scatter.4
